TPU v7x, 32 devices: a whole 2x2x4 slice. The times are simulated.
32 devices in a mesh: ep: 8 (over z, y), tp: 4 (over x, core).
Axes of the slice: x: 2, y: 2, z: 4, core: 2. Of those that a mesh axis runs over, the one named last changes fastest.
Arguments:
- tokens: bfloat16 [128, 2048], P('ep', 'tp'), may hold values from -40 to 40
- kv_cache: bfloat16 [128, 1024, 512], P('ep', None, 'tp'), may hold values from -1000 to 1000
- cum_gate: float32 [128, 16, 1024], P('ep', 'tp'), may hold values from -400 to 0, as said below
- lengths: int32 [128], P('ep'), may hold values from 256 to 1024
- w_query: bfloat16 [2048, 1024], P(None, 'tp'), may hold values from -0.125 to 0.125
- w_key: bfloat16 [2048, 256], P(None, 'tp'), may hold values from -0.125 to 0.125
- w_value: bfloat16 [2048, 256], P(None, 'tp'), may hold values from -0.125 to 0.125
- w_forget: bfloat16 [2048, 16], P(None, 'tp'), may hold values from -0.5 to 0.5
- forget_bias: float32 [16], P('tp'), may hold values from -2.5 to 1.5
- w_out: bfloat16 [1024, 2048], P('tp'), may hold values from -0.1875 to 0.1875
- attn_gain: bfloat16 [2048], replicated, may hold values from 0.099609375 to 1.8984375
- ffn_gain: bfloat16 [2048], replicated, may hold values from 0.099609375 to 1.8984375
- mix_gate: bfloat16 [2048], replicated, may hold values from -0.125 to 0.125
- expert_gate: bfloat16 [8, 2048, 1024], P('ep', None, 'tp'), may hold values from -0.125 to 0.125
- expert_up: bfloat16 [8, 2048, 1024], P('ep', None, 'tp'), may hold values from -0.125 to 0.125
- expert_down: bfloat16 [8, 1024, 2048], P('ep', 'tp'), may hold values from -0.1875 to 0.1875
- chosen: int32 [128, 2], P('ep'), may hold values from 0 to 7, as said below
- route_weight: float32 [128, 2], P('ep'), may hold values from 0.5 to 1.5
- dense_gate: bfloat16 [2048, 1024], P(None, 'tp'), may hold values from -0.125 to 0.125
- dense_up: bfloat16 [2048, 1024], P(None, 'tp'), may hold values from -0.125 to 0.125
- dense_down: bfloat16 [1024, 2048], P('tp'), may hold values from -0.1875 to 0.1875
Outputs:
- mixed: bfloat16 [128, 2048], P('ep', 'tp')
Inputs may be any that keep to these rules, and one draw needn't show every extreme that they name: `cum_gate`: along positions each row never rises: entry p is the sum of the log forget gates of positions 0 to p of that sequence and head. `chosen`: each row names two different experts of one group of 8 consecutive expert numbers. The rows of one device name any one expert at most 8 times, and some expert exactly 8 times.
All inputs are finite; a program needn't handle non-finite values.
Results may differ from a plain program's by a relative error of at most 0.014.
Values may be sent and summed in bfloat16 or wider, within the bound.
A program may use at most 64 MiB of HBM per device.

v0:
```python
import jax
import jax.numpy as jnp
from jax import lax
from jax.sharding import PartitionSpec as P

HD = 64
TOP = 2


epsilon = 1e-06


def norm_rows(values, scales):
    widened = values.astype(jnp.float32)
    square = jnp.mean(widened * widened, axis=-1, keepdims=True)
    return (widened * lax.rsqrt(square + epsilon) * scales.astype(jnp.float32)).astype(jnp.bfloat16)


def attend(h_one, kv_cache, cum_gate, lengths, w_query, w_key, w_value, w_forget, forget_bias):
    tok_count = h_one.shape[0]
    cache_len = kv_cache.shape[1]
    kv_local = w_key.shape[1] // HD
    q_local = w_query.shape[1] // HD
    group_size = q_local // kv_local
    score_scale = HD ** (-0.5)
    queries = jnp.dot(h_one, w_query, preferred_element_type=jnp.float32).astype(jnp.bfloat16)
    queries = queries.reshape(tok_count, kv_local, group_size, HD)
    key_new = jnp.dot(h_one, w_key, preferred_element_type=jnp.float32).astype(jnp.bfloat16)
    key_new = key_new.reshape(tok_count, kv_local, HD)
    value_new = jnp.dot(h_one, w_value, preferred_element_type=jnp.float32).astype(jnp.bfloat16)
    value_new = value_new.reshape(tok_count, kv_local, HD)
    forget_now = jax.nn.log_sigmoid(
        jnp.dot(h_one, w_forget, preferred_element_type=jnp.float32) + forget_bias
    )
    forget_now = forget_now.reshape(tok_count, kv_local, group_size)
    stacked = kv_cache.reshape(tok_count, cache_len, kv_local, 2, HD)
    past_keys = stacked[:, :, :, 0, :]
    past_values = stacked[:, :, :, 1, :]
    scores = (
        jnp.einsum("sjgd,scjd->sjgc", queries, past_keys, preferred_element_type=jnp.float32)
        * score_scale
    )
    cumulative = cum_gate.reshape(tok_count, kv_local, group_size, cache_len)
    position_rows = jnp.arange(cache_len, dtype=jnp.int32)
    at_last = (position_rows[None, :] == (lengths - 1)[:, None]).astype(jnp.float32)
    latest = jnp.sum(cumulative * at_last[:, None, None, :], axis=-1, keepdims=True)
    scores = scores + latest - cumulative + forget_now[:, :, :, None]
    inside = position_rows[None, :] < lengths[:, None]
    scores = jnp.where(inside[:, None, None, :], scores, -jnp.inf)
    own_score = (
        jnp.einsum("sjgd,sjd->sjg", queries, key_new, preferred_element_type=jnp.float32)
        * score_scale
    )
    highest = jnp.maximum(jnp.max(scores, axis=-1), own_score)
    weights = jnp.exp(scores - highest[:, :, :, None])
    own_weight = jnp.exp(own_score - highest)
    denominator = jnp.sum(weights, axis=-1) + own_weight
    weights = (weights / denominator[:, :, :, None]).astype(jnp.bfloat16)
    own_weight = (own_weight / denominator).astype(jnp.bfloat16)
    blended = jnp.einsum(
        "sjgc,scjd->sjgd", weights, past_values, preferred_element_type=jnp.float32
    )
    blended = (
        blended
        + own_weight.astype(jnp.float32)[:, :, :, None]
        * value_new.astype(jnp.float32)[:, :, None, :]
    )
    return blended.astype(jnp.bfloat16).reshape(tok_count, q_local * HD)


def local(
    tokens,
    kv_cache,
    cum_gate,
    lengths,
    w_query,
    w_key,
    w_value,
    w_forget,
    forget_bias,
    w_out,
    attn_gain,
    ffn_gain,
    mix_gate,
    expert_gate,
    expert_up,
    expert_down,
    chosen,
    route_weight,
    dense_gate,
    dense_up,
    dense_down,
):
    tok_count = tokens.shape[0]
    slice_width = tokens.shape[1]
    ep_count = lax.axis_size("ep")
    gathered = lax.all_gather(tokens, "tp", axis=1, tiled=True)
    model_width = gathered.shape[1]
    h_one = norm_rows(gathered, attn_gain)
    head_out = attend(
        h_one, kv_cache, cum_gate, lengths, w_query, w_key, w_value, w_forget, forget_bias
    )
    partial_value = jnp.dot(head_out, w_out, preferred_element_type=jnp.float32)
    tp_offset = lax.axis_index("tp") * slice_width
    attention = lax.psum(partial_value.astype(jnp.bfloat16), "tp").astype(jnp.float32)
    residual_full = (gathered.astype(jnp.float32) + attention).astype(jnp.bfloat16)
    h_two = norm_rows(residual_full, ffn_gain)
    residual = lax.dynamic_slice_in_dim(residual_full, tp_offset, slice_width, 1)
    capacity = max(2, (4 * tok_count + ep_count - 1) // ep_count)
    routes = chosen.reshape(-1)
    expert_ids = jnp.arange(ep_count, dtype=jnp.int32)
    one_hot = (routes[:, None] == expert_ids[None, :]).astype(jnp.int32)
    rank_of = jnp.sum((jnp.cumsum(one_hot, axis=0) - one_hot) * one_hot, axis=1)
    slot_of = routes * capacity + rank_of
    slot_ids = jnp.arange(ep_count * capacity, dtype=jnp.int32)
    chooser = (slot_ids[:, None] == slot_of[None, :]).astype(jnp.bfloat16)
    per_token = jnp.sum(chooser.reshape(ep_count * capacity, tok_count, TOP), axis=2)
    outgoing = jnp.dot(per_token, h_two, preferred_element_type=jnp.float32).astype(jnp.bfloat16)
    outgoing = outgoing.reshape(ep_count, capacity, model_width)
    received = lax.all_to_all(outgoing, "ep", split_axis=0, concat_axis=0, tiled=True)
    flat_rows = received.reshape(-1, model_width)
    gate_pre = jnp.dot(flat_rows, expert_gate[0], preferred_element_type=jnp.float32)
    up_pre = jnp.dot(flat_rows, expert_up[0], preferred_element_type=jnp.float32)
    hidden = (jax.nn.silu(gate_pre) * up_pre).astype(jnp.bfloat16)
    part_out = jnp.dot(hidden, expert_down[0], preferred_element_type=jnp.float32)
    summed = lax.psum_scatter(part_out.astype(jnp.bfloat16), "tp", scatter_dimension=1, tiled=True)
    shares = summed.reshape(received.shape[0], received.shape[1], -1)
    returned = lax.all_to_all(shares, "ep", split_axis=0, concat_axis=0, tiled=True)
    returned = returned.reshape(ep_count * capacity, slice_width)
    picked = jnp.dot(chooser.T, returned, preferred_element_type=jnp.float32)
    routed_sum = jnp.sum(
        picked.reshape(tok_count, TOP, slice_width) * route_weight[:, :, None], axis=1
    )
    dense_pre = jnp.dot(h_two, dense_gate, preferred_element_type=jnp.float32)
    dense_lift = jnp.dot(h_two, dense_up, preferred_element_type=jnp.float32)
    dense_act = (jax.nn.silu(dense_pre) * dense_lift).astype(jnp.bfloat16)
    dense_part = jnp.dot(dense_act, dense_down, preferred_element_type=jnp.float32)
    dense_out = lax.psum_scatter(
        dense_part.astype(jnp.bfloat16), "tp", scatter_dimension=1, tiled=True
    ).astype(jnp.float32)
    blend_gate = jax.nn.sigmoid(jnp.dot(h_two, mix_gate, preferred_element_type=jnp.float32))
    return (residual.astype(jnp.float32) + routed_sum + blend_gate[:, None] * dense_out).astype(
        jnp.bfloat16
    )


def solution(mesh):
    in_specs = (
        P("ep", "tp"),
        P("ep", None, "tp"),
        P("ep", "tp", None),
        P("ep"),
        P(None, "tp"),
        P(None, "tp"),
        P(None, "tp"),
        P(None, "tp"),
        P("tp"),
        P("tp", None),
        P(),
        P(),
        P(),
        P("ep", None, "tp"),
        P("ep", None, "tp"),
        P("ep", "tp", None),
        P("ep", None),
        P("ep", None),
        P(None, "tp"),
        P(None, "tp"),
        P("tp", None),
    )
    out_specs = P("ep", "tp")
    return jax.shard_map(local, mesh=mesh, in_specs=in_specs, out_specs=out_specs, check_vma=False)
```

profile of v0, /device:TPU:0, one launch (start us, length us, event | category | flops | bytes accessed | tf_op | source)
XLA Modules:
  0.0 130.5 jit_solution(5122951195548866926)
XLA Ops:
  6.5 6.6 %all_gather.3 = bf16[16,2048]{1,0:T(8,128)(2,1)S(1)} all-gather(bf16[16,512]{1,0:T(8,128)(2,1)} %param.21), channel_id=1, replica_groups=mesh['ep'=8,'tp'=4] {'tp'}, dimensions={1}, use_global_device_ids=true | all-gather | bytes 81920 | tf_op jit(solution)/shard_map/all_gather | solution.py:97
  13.1 0.1 fusion.34
  13.3 0.7 convert_element_type.98
  13.9 1.5 %convolution_convert_fusion.4 = bf16[16,256]{1,0:T(8,128)(2,1)S(1)} fusion(bf16[2048,256]{1,0:T(8,128)(2,1)} %param.25, bf16[16,2048]{1,0:T(8,128)(2,1)S(1)} %all_gather.3, f32[2048]{0:T(1024)S(1)} %convert_element_type.98, f32[16]{0:T(128)S(1)} %add_rsqrt_fusion.1), kind=kOutput, calls=%fused_computation.23 | convolution fusion | flops 16912384 | bytes 1130560 | tf_op jit(solution)/shard_map/dot_general | solution.py:26
  15.5 0.1 reshape.204
  15.6 6.5 %copy.43 = bf16[16,1024,128]{1,2,0:T(8,128)(2,1)} copy(bf16[16,1024,128]{2,1,0:T(8,128)(2,1)} %param.22) | data formatting | bytes 8388608 | tf_op args[1]
  22.1 0.2 fusion.63
  22.3 0.1 copy.45
  22.4 0.1 iota_compare_fusion.1
  22.5 0.2 fusion.15
  22.7 2.2 %fusion.8 = f32[16,4,1024]{2,1,0:T(4,128)S(1)} fusion(bf16[16,4,64]{2,1,0:T(4,128)(2,1)S(1)} %reshape.204, bf16[16,1024,1,2,64]{1,4,3,0,2:T(8,128)(2,1)} %bitcast.68), kind=kOutput, calls=%fused_computation.14 | convolution fusion | flops 8454144 | bytes 2367488 | tf_op jit(solution)/shard_map/sjgd,scjd->sjgc/dot_general | solution.py:40
  24.9 0.1 fusion.59
  25.1 0.3 fusion.77
  25.4 0.2 fusion.30
  25.7 0.2 fusion.14
  25.9 0.7 fusion.12
  26.6 0.1 reshape.208
  26.7 2.2 %convolution_convert_fusion.3 = bf16[16,2048]{1,0:T(8,128)(2,1)} fusion(bf16[16,256]{1,0:T(8,128)(2,1)S(1)} %reshape.208, bf16[256,2048]{1,0:T(8,128)(2,1)} %param.30), kind=kOutput, calls=%fused_computation.5 | convolution fusion | flops 16809984 | bytes 1122304 | tf_op jit(solution)/shard_map/dot_general | solution.py:103
  29.0 0.0 all-reduce.2.cloned.1.call-update
  29.0 0.1 copy.47
  29.1 0.1 reshape.209
  29.2 0.1 fusion.54
  29.2 0.1 reduce_window_sum.11
  29.3 0.2 select_reduce_fusion
  29.5 0.1 reduce_sum.72
  29.6 0.1 copy.48
  29.7 0.1 fusion.57
  29.8 32.6 %all-reduce.2.cloned.1.call-done = bf16[16,2048]{1,0:T(8,128)(2,1)} async-done(((bf16[16,2048]{1,0:T(8,128)(2,1)}), bf16[16,2048]{1,0:T(8,128)(2,1)}) %all-reduce.2.cloned.1.call-update) | async-done | bytes 65552 | tf_op jit(solution)/shard_map/psum | solution.py:105
  62.4 1.0 fusion.31
  63.4 1.0 fusion.1
  64.3 5.5 %all-to-all-start = ((bf16[8,8,2048]{2,1,0:T(8,128)(2,1)}), bf16[8,8,2048]{2,1,0:T(8,128)(2,1)S(1)}, u32[]{:S(2)}, u32[]{:S(2)}) async-start(bf16[8,8,2048]{2,1,0:T(8,128)(2,1)} %fusion.1), calls=%async_computation | async-start | bytes 524288 | tf_op jit(solution)/shard_map/all_to_all | solution.py:120
  69.9 0.0 reduce-scatter.3.cloned.1.call-start
  69.9 0.6 reshape.217
  70.5 0.1 iota_compare_fusion.4
  70.6 7.5 %all-to-all-done = bf16[8,8,2048]{2,1,0:T(8,128)(2,1)S(1)} async-done(((bf16[8,8,2048]{2,1,0:T(8,128)(2,1)}), bf16[8,8,2048]{2,1,0:T(8,128)(2,1)S(1)}, u32[]{:S(2)}, u32[]{:S(2)}) %all-to-all-start) | async-done | bytes 262176 | tf_op jit(solution)/shard_map/all_to_all | solution.py:120
  78.1 1.5 %fusion.24 = f32[64,256]{1,0:T(8,128)S(1)} fusion(bf16[1,2048,256]{2,1,0:T(8,128)(2,1)} %param.34, bf16[8,8,2048]{2,1,0:T(8,128)(2,1)S(1)} %all-to-all-done), kind=kOutput, calls=%fused_computation.37 | convolution fusion | flops 67108864 | bytes 1376256 | tf_op jit(solution)/shard_map/dot_general | solution.py:122
  79.6 2.7 %convolution_convert_fusion = bf16[64,2048]{1,0:T(8,128)(2,1)} fusion(bf16[1,256,2048]{2,1,0:T(8,128)(2,1)S(1)} %copy-done, bf16[1,2048,256]{2,1,0:T(8,128)(2,1)} %param.35, bf16[8,8,2048]{2,1,0:T(8,128)(2,1)S(1)} %all-to-all-done, f32[64,256]{1,0:T(8,128)S(1)} %fusion.24), kind=kOutput, calls=%fused_computation.1 | convolution fusion | flops 134447104 | bytes 2686976 | tf_op jit(solution)/shard_map/dot_general | solution.py:125
  82.3 0.0 reduce-scatter.3.cloned.1.call-update
  82.4 0.0 reduce-scatter.5.cloned.1.call-start
  82.4 1.5 %fusion.72 = f32[16,256]{1,0:T(8,128)S(1)} fusion(bf16[2048,256]{1,0:T(8,128)(2,1)} %param.39, bf16[16,2048]{1,0:T(8,128)(2,1)S(1)} %get-tuple-element.6, f32[2048]{0:T(1024)S(1)} %convert_element_type.116, f32[16]{0:T(128)} %copy-done.4), kind=kOutput, calls=%fused_computation.102 | convolution fusion | flops 16908288 | bytes 1138752 | tf_op jit(solution)/shard_map/dot_general | solution.py:134
  83.9 2.0 %convolution_convert_fusion.2 = bf16[16,2048]{1,0:T(8,128)(2,1)} fusion(bf16[256,2048]{1,0:T(8,128)(2,1)S(1)} %copy-done.2, bf16[2048,256]{1,0:T(8,128)(2,1)S(1)} %copy-done.3, f32[16,256]{1,0:T(8,128)S(1)} %fusion.72, bf16[16,2048]{1,0:T(8,128)(2,1)S(1)} %get-tuple-element.6, f32[2048]{0:T(1024)S(1)} %convert_element_type.116, f32[16]{0:T(128)} %copy-done.4), kind=kOutput, calls=%fused_computation.4 | convolution fusion | flops 33742848 | bytes 2252864 | tf_op jit(solution)/shard_map/dot_general | solution.py:137
  86.0 14.6 %reduce-scatter.3.cloned.1.call-done = bf16[64,512]{1,0:T(8,128)(2,1)} async-done(((bf16[64,2048]{1,0:T(8,128)(2,1)}), bf16[64,512]{1,0:T(8,128)(2,1)}) %reduce-scatter.3.cloned.1.call-update) | async-done | bytes 65552 | tf_op jit(solution)/shard_map/reduce_scatter | solution.py:126
  100.5 5.5 %all-to-all-start.1 = ((bf16[8,8,512]{2,1,0:T(8,128)(2,1)}), bf16[8,8,512]{2,1,0:T(8,128)(2,1)S(1)}, u32[]{:S(2)}, u32[]{:S(2)}) async-start(bf16[8,8,512]{2,1,0:T(8,128)(2,1)} %bitcast.70), calls=%async_computation.2 | async-start | bytes 131072 | tf_op jit(solution)/shard_map/all_to_all | solution.py:128
  106.0 0.9 fusion.20
  106.9 6.0 %all-to-all-done.1 = bf16[8,8,512]{2,1,0:T(8,128)(2,1)S(1)} async-done(((bf16[8,8,512]{2,1,0:T(8,128)(2,1)}), bf16[8,8,512]{2,1,0:T(8,128)(2,1)S(1)}, u32[]{:S(2)}, u32[]{:S(2)}) %all-to-all-start.1) | async-done | bytes 65568 | tf_op jit(solution)/shard_map/all_to_all | solution.py:128
  112.9 0.8 fusion.10
  113.8 8.8 %reduce-scatter.5.cloned.1.call-done = bf16[16,512]{1,0:T(8,128)(2,1)} async-done(((bf16[16,2048]{1,0:T(8,128)(2,1)}), bf16[16,512]{1,0:T(8,128)(2,1)}) %reduce-scatter.5.cloned.1.call-update) | async-done | bytes 16400 | tf_op jit(solution)/shard_map/reduce_scatter | solution.py:138
  122.5 1.4 %add_convert_fusion = bf16[16,512]{1,0:T(8,128)(2,1)} fusion(bf16[16,512]{1,0:T(8,128)(2,1)} %reduce-scatter.5.cloned.1.call-done, f32[16,512]{1,0:T(8,128)S(1)} %fusion.10, f32[16]{0:T(128)S(1)} %fusion.20, bf16[16,2048]{1,0:T(8,128)(2,1)S(1)} %get-tuple-element.6, s32[]{:T(128)S(6)} %select_n.15), kind=kLoop, calls=%fused_computation.70 | loop fusion | flops 49152 | bytes 81988 | tf_op jit(solution)/shard_map/convert_element_type | solution.py:142
  (39 shorter events, 0.2 us)
Async XLA Ops:
  6.5 73.1 %copy-start = (bf16[1,256,2048]{2,1,0:T(8,128)(2,1)S(1)}, bf16[1,256,2048]{2,1,0:T(8,128)(2,1)}, u32[]{:S(2)}) copy-start(bf16[1,256,2048]{2,1,0:T(8,128)(2,1)} %param.36) | copy-start | bytes 3145732
  6.5 55.8 %all-reduce.2.cloned.1.call-start = ((), (), s32[]{:S(2)}) async-start(), calls=%async_computation.4 | async-start | bytes 131072 | tf_op jit(solution)/shard_map/psum | solution.py:105
  15.5 6.5 %copy-start.12 = (bf16[2048,4]{0,1:T(4,128)(2,1)S(1)}, bf16[2048,4]{0,1:T(4,128)(2,1)}, u32[]{:S(2)}) copy-start(bf16[2048,4]{0,1:T(4,128)(2,1)} %param.28) | copy-start | bytes 49156
  15.6 6.5 %copy-start.13 = (f32[4]{0:T(128)S(1)}, f32[4]{0:T(128)}, u32[]{:S(2)}) copy-start(f32[4]{0:T(128)} %param.29) | copy-start | bytes 52
  15.6 6.8 %copy-start.8 = (s32[16]{0:T(128)S(1)}, s32[16]{0:T(128)}, u32[]{:S(2)}) copy-start(s32[16]{0:T(128)} %param.24) | copy-start | bytes 196
  15.6 6.9 %copy-start.9 = (bf16[2048,64]{0,1:T(8,128)(2,1)S(1)}, bf16[2048,64]{0,1:T(8,128)(2,1)}, u32[]{:S(2)}) copy-start(bf16[2048,64]{0,1:T(8,128)(2,1)} %param.26) | copy-start | bytes 786436
  15.6 9.5 %copy-start.10 = (f32[16,4,1024]{2,1,0:T(4,128)S(1)}, f32[16,4,1024]{2,1,0:T(4,128)}, u32[]{:S(2)}) copy-start(f32[16,4,1024]{2,1,0:T(4,128)} %param.23) | copy-start | bytes 786436
  22.1 3.6 %copy-start.11 = (bf16[2048,64]{0,1:T(8,128)(2,1)S(1)}, bf16[2048,64]{0,1:T(8,128)(2,1)}, u32[]{:S(2)}) copy-start(bf16[2048,64]{0,1:T(8,128)(2,1)} %param.27) | copy-start | bytes 786436
  22.4 3.5 %copy-start.1 = (bf16[16,1024,128]{1,2,0:T(8,128)(2,1)S(1)}, bf16[16,1024,128]{1,2,0:T(8,128)(2,1)}, u32[]{:S(2)}) copy-start(bf16[16,1024,128]{1,2,0:T(8,128)(2,1)} %copy.43) | copy-start | bytes 12582916
  24.9 4.1 %copy-start.7 = (s32[16,2]{0,1:T(2,128)S(1)}, s32[16,2]{0,1:T(2,128)}, u32[]{:S(2)}) copy-start(s32[16,2]{0,1:T(2,128)} %param.37) | copy-start | bytes 388
  24.9 4.8 %copy-start.5 = (bf16[2048]{0:T(1024)(128)(2,1)S(1)}, bf16[2048]{0:T(1024)(128)(2,1)}, u32[]{:S(2)}) copy-start(bf16[2048]{0:T(1024)(128)(2,1)} %param.32) | copy-start | bytes 12292
  25.1 44.8 %copy-start.6 = (bf16[2048]{0:T(1024)(128)(2,1)S(1)}, bf16[2048]{0:T(1024)(128)(2,1)}, u32[]{:S(2)}) copy-start(bf16[2048]{0:T(1024)(128)(2,1)} %param.33) | copy-start | bytes 12292
  26.6 57.3 %copy-start.2 = (bf16[256,2048]{1,0:T(8,128)(2,1)S(1)}, bf16[256,2048]{1,0:T(8,128)(2,1)}, u32[]{:S(2)}) copy-start(bf16[256,2048]{1,0:T(8,128)(2,1)} %param.41) | copy-start | bytes 3145732
  26.6 57.3 %copy-start.3 = (bf16[2048,256]{1,0:T(8,128)(2,1)S(1)}, bf16[2048,256]{1,0:T(8,128)(2,1)}, u32[]{:S(2)}) copy-start(bf16[2048,256]{1,0:T(8,128)(2,1)} %param.40) | copy-start | bytes 3145732
  63.4 1.0 copy-start.4
  64.3 13.7 %all-to-all-start = ((bf16[8,8,2048]{2,1,0:T(8,128)(2,1)}), bf16[8,8,2048]{2,1,0:T(8,128)(2,1)S(1)}, u32[]{:S(2)}, u32[]{:S(2)}) async-start(bf16[8,8,2048]{2,1,0:T(8,128)(2,1)} %fusion.1), calls=%async_computation | async-start | bytes 524288 | tf_op jit(solution)/shard_map/all_to_all | solution.py:120
  69.9 30.7 %reduce-scatter.3.cloned.1.call-start = ((), (), s32[]{:S(2)}) async-start(), calls=%async_computation.5 | async-start | bytes 327680 | tf_op jit(solution)/shard_map/reduce_scatter | solution.py:126
  82.4 40.2 %reduce-scatter.5.cloned.1.call-start = ((), (), s32[]{:S(2)}) async-start(), calls=%async_computation.6 | async-start | bytes 81920 | tf_op jit(solution)/shard_map/reduce_scatter | solution.py:138
  100.5 12.4 %all-to-all-start.1 = ((bf16[8,8,512]{2,1,0:T(8,128)(2,1)}), bf16[8,8,512]{2,1,0:T(8,128)(2,1)S(1)}, u32[]{:S(2)}, u32[]{:S(2)}) async-start(bf16[8,8,512]{2,1,0:T(8,128)(2,1)} %bitcast.70), calls=%async_computation.2 | async-start | bytes 131072 | tf_op jit(solution)/shard_map/all_to_all | solution.py:128
Sparse Core Ops, SparseCore 0:
  29.1 33.2 all-reduce.1
  82.5 18.0 reduce-scatter.2
  103.0 19.5 reduce-scatter.4
where the time goes:
time: 131 us; the launch traced here: 130 us
  waiting for transfers between devices  69.4 us (53%)
  matrix products  17.9 us (14%)
  between operations  13.3 us (10%)
  starting transfers between devices  11.1 us (8%)
  local copies, waits for them, and re-layouts  7.77 us (6%)
  blocking collectives  6.57 us (5%)
  other arithmetic  4.38 us (3%)
    psum x1, waiting for transfers between devices, local(): lax.psum(partial_value.astype(jnp.bfloat16), 'tp').astype(jnp.float32)  32.6 us
    reduce_scatter x1, waiting for transfers between devices, local(): lax.psum_scatter(part_out.astype(jnp.bfloat16), 'tp', scatter_dimension=1...  14.6 us
    reduce_scatter x1, waiting for transfers between devices, local(): lax.psum_scatter(dense_part.astype(jnp.bfloat16), 'tp', scatter_dimension...  8.77 us
    all_to_all x1, waiting for transfers between devices, local(): lax.all_to_all(outgoing, 'ep', split_axis=0, concat_axis=0, tiled=True)  7.45 us
    unnamed x31, local copies, waits for them, and re-layouts  7.22 us
    all_gather x1, blocking collectives, local(): gathered = lax.all_gather(tokens, 'tp', axis=1, tiled=True)  6.57 us
    all_to_all x1, waiting for transfers between devices, local(): lax.all_to_all(shares, 'ep', split_axis=0, concat_axis=0, tiled=True)  6 us
    all_to_all x1, starting transfers between devices, local(): lax.all_to_all(outgoing, 'ep', split_axis=0, concat_axis=0, tiled=True)  5.52 us
  transfers between devices with their start and end apart: 5, of which 5 were waited for; matrix products, arithmetic and copies ran while one was open for 5% of the time, Pallas kernels for 0%

commit v1 on v0

v1 whole, which is shorter than its diff:
```python
import functools

import jax
import jax.numpy as jnp
from jax import lax
from jax.experimental import pallas as pl
from jax.experimental.pallas import tpu as pltpu
from jax.sharding import PartitionSpec as P

HD = 64
TOP = 2
MESH = pl.DeviceIdType.MESH
F32 = jnp.float32
BF16 = jnp.bfloat16
epsilon = 1e-06


def dot(a, b):
    return jnp.dot(a, b, preferred_element_type=F32)


def norm_rows(widened, scales):
    square = jnp.mean(widened * widened, axis=-1, keepdims=True)
    return (widened * lax.rsqrt(square + epsilon) * scales.astype(F32)).astype(BF16)


def kernel(
    n_ep,
    n_tp,
    cap,
    tokens,
    lengths,
    forget_bias,
    attn_gain,
    ffn_gain,
    mix_gate,
    chosen,
    route_weight,
    kv_hbm,
    cum_hbm,
    wq_hbm,
    wk_hbm,
    wv_hbm,
    wf_hbm,
    wo_hbm,
    eg_hbm,
    eu_hbm,
    ed_hbm,
    dg_hbm,
    du_hbm,
    dd_hbm,
    out,
    kv,
    cum,
    wq,
    wk,
    wv,
    wf,
    wo,
    eg,
    eu,
    ed,
    dg,
    du,
    dd,
    load_sem,
    kv_sem,
    gathered,
    q3,
    f3,
    kvn,
    o3,
    att_out,
    att_in,
    disp_out,
    disp_in,
    dense_send,
    dense_recv,
    exp_send,
    exp_recv,
    ret_out,
    ret_in,
    tp_send,
    tp_recv,
    ep_send,
    ep_recv,
):
    me_tp = lax.axis_index("tp")
    me_ep = lax.axis_index("ep")
    seqs, width = tokens.shape
    heads = cum.shape[1]
    cache_len = kv.shape[1]
    rows = n_ep * cap

    loads = {}
    for spot, (name, src, dst) in enumerate(
        (
            ("wq", wq_hbm, wq),
            ("wk", wk_hbm, wk),
            ("wv", wv_hbm, wv),
            ("wf", wf_hbm, wf),
            ("cum", cum_hbm, cum),
        )
    ):
        loads[name] = pltpu.make_async_copy(src, dst, load_sem.at[spot])
        loads[name].start()
    kv_parts = kv_sem.shape[0]
    part = seqs // kv_parts
    kv_loads = []
    for piece in range(kv_parts):
        span = pl.ds(piece * part, part)
        kv_loads.append(
            pltpu.make_async_copy(kv_hbm.at[span], kv.at[span], kv_sem.at[piece])
        )
        kv_loads[-1].start()
    for spot, (name, src, dst) in enumerate(
        (
            ("wo", wo_hbm, wo),
            ("dg", dg_hbm, dg),
            ("du", du_hbm, du),
            ("dd", dd_hbm, dd),
            ("eg", eg_hbm.at[0], eg),
            ("eu", eu_hbm.at[0], eu),
            ("ed", ed_hbm.at[0], ed),
        )
    ):
        loads[name] = pltpu.make_async_copy(src, dst, load_sem.at[5 + spot])
        loads[name].start()

    barrier = pltpu.get_barrier_semaphore()
    for step in range(1, n_tp):
        pl.semaphore_signal(
            barrier,
            inc=1,
            device_id={"tp": lax.rem(me_tp + step, n_tp)},
            device_id_type=MESH,
        )

    def greet(step, carry):
        pl.semaphore_signal(
            barrier,
            inc=1,
            device_id={"ep": lax.rem(me_ep + step, n_ep)},
            device_id_type=MESH,
        )
        return carry

    lax.fori_loop(1, n_ep, greet, 0)
    pl.semaphore_wait(barrier, n_tp - 1 + n_ep - 1)

    def tp_copy(phase, step, src, dst):
        return pltpu.make_async_remote_copy(
            src_ref=src,
            dst_ref=dst,
            send_sem=tp_send.at[phase, step],
            recv_sem=tp_recv.at[phase, step],
            device_id={"tp": lax.rem(me_tp + step, n_tp)},
            device_id_type=MESH,
        )

    def ep_copy(phase, step, src, dst):
        return pltpu.make_async_remote_copy(
            src_ref=src,
            dst_ref=dst,
            send_sem=ep_send.at[phase, step],
            recv_sem=ep_recv.at[phase, step],
            device_id={"ep": lax.rem(me_ep + step, n_ep)},
            device_id_type=MESH,
        )

    token_copies = [
        tp_copy(0, step, tokens, gathered.at[me_tp]) for step in range(1, n_tp)
    ]
    for copy in token_copies:
        copy.start()
    gathered[me_tp] = tokens[...]

    slot = lax.broadcasted_iota(jnp.int32, (seqs, rows), 1)
    slot_expert = slot // cap
    slot_place = (slot % cap).astype(F32)
    first = (chosen[:, 0:1] == slot_expert).astype(F32)
    second = (chosen[:, 1:2] == slot_expert).astype(F32)
    either = first + second
    earlier = (
        lax.broadcasted_iota(jnp.int32, (seqs, seqs), 1)
        < lax.broadcasted_iota(jnp.int32, (seqs, seqs), 0)
    ).astype(F32)
    rank = dot(earlier.astype(BF16), either.astype(BF16))
    in_place = (rank == slot_place).astype(F32)
    first = (first * in_place).astype(BF16)
    second = (second * in_place).astype(BF16)
    either = either * in_place

    for copy in token_copies:
        copy.wait()
    tokens_full = jnp.concatenate(
        [gathered[member].astype(F32) for member in range(n_tp)], axis=1
    )
    h_one = norm_rows(tokens_full, attn_gain[...])

    for name in ("wq", "wk", "wv", "wf"):
        loads[name].wait()
    queries = dot(h_one, wq[...]).astype(BF16).astype(F32)
    key_new = dot(h_one, wk[...]).astype(BF16).astype(F32)
    value_new = dot(h_one, wv[...]).astype(BF16).astype(F32)
    forget_pre = dot(h_one, wf[...]) + forget_bias[...]
    forget_now = jnp.minimum(forget_pre, 0.0) - jnp.log1p(
        jnp.exp(-jnp.abs(forget_pre))
    )
    blank = jnp.zeros((seqs, HD), F32)
    for head in range(heads):
        q3[:, head, :] = jnp.concatenate(
            [queries[:, head * HD : (head + 1) * HD], blank], axis=1
        )
        f3[:, head, :] = jnp.broadcast_to(forget_now[:, head : head + 1], (seqs, 2 * HD))
    kvn[...] = jnp.concatenate([key_new, value_new], axis=1)

    score_scale = HD ** (-0.5)
    position = lax.broadcasted_iota(jnp.int32, (heads, cache_len), 1)
    loads["cum"].wait()

    def attend(seq):
        length = lengths[seq]
        query = q3[seq]
        entries = kv[seq]
        scores = (
            lax.dot_general(
                query.astype(BF16),
                entries,
                (((1,), (1,)), ((), ())),
                preferred_element_type=F32,
            )
            * score_scale
        )
        gates = cum[seq]
        latest = jnp.sum(
            jnp.where(position == length - 1, gates, 0.0), axis=1, keepdims=True
        )
        scores = scores - gates + (latest + f3[seq][:, 0:1])
        scores = jnp.where(position < length, scores, -jnp.inf)
        new_row = kvn[pl.ds(seq, 1), :]
        own_score = jnp.sum(query * new_row, axis=1, keepdims=True) * score_scale
        highest = jnp.maximum(jnp.max(scores, axis=1, keepdims=True), own_score)
        weights = jnp.exp(scores - highest)
        own_weight = jnp.exp(own_score - highest)
        inverse = 1.0 / (jnp.sum(weights, axis=1, keepdims=True) + own_weight)
        blended = dot((weights * inverse).astype(BF16), entries)
        own_weight = (own_weight * inverse).astype(BF16).astype(F32)
        o3[seq] = blended + own_weight * new_row

    for piece in range(kv_parts):
        kv_loads[piece].wait()
        for seq in range(piece * part, (piece + 1) * part):
            attend(seq)
    head_out = jnp.concatenate(
        [o3[:, head, :][:, HD:] for head in range(heads)], axis=1
    ).astype(BF16)

    loads["wo"].wait()
    att_out[...] = dot(head_out, wo[...]).astype(BF16)
    att_copies = [tp_copy(1, step, att_out, att_in.at[step]) for step in range(1, n_tp)]
    for copy in att_copies:
        copy.start()
    attention = att_out[...].astype(F32)
    for step in range(1, n_tp):
        att_copies[step - 1].wait()
        attention = attention + att_in[step].astype(F32)
    residual_full = (tokens_full + attention).astype(BF16)
    h_two = norm_rows(residual_full.astype(F32), ffn_gain[...])
    for member in range(n_tp):
        gathered[member] = residual_full[:, member * width : (member + 1) * width]

    outgoing = dot(jnp.transpose(either).astype(BF16), h_two)
    disp_out[...] = outgoing.reshape(n_ep, cap, n_tp * width).astype(BF16)

    def dispatch(step, carry):
        ep_copy(
            0, step, disp_out.at[lax.rem(me_ep + step, n_ep)], disp_in.at[me_ep]
        ).start()
        return carry

    lax.fori_loop(1, n_ep, dispatch, 0)
    disp_in[me_ep] = disp_out[me_ep]

    for name in ("dg", "du", "dd"):
        loads[name].wait()
    dense_pre = dot(h_two, dg[...])
    dense_act = (dense_pre * jax.nn.sigmoid(dense_pre) * dot(h_two, du[...])).astype(BF16)
    dense_part = dot(dense_act, dd[...]).astype(BF16)
    for member in range(n_tp):
        dense_send[member] = dense_part[:, member * width : (member + 1) * width]
    dense_copies = [
        tp_copy(
            2, step, dense_send.at[lax.rem(me_tp + step, n_tp)], dense_recv.at[step]
        )
        for step in range(1, n_tp)
    ]
    for copy in dense_copies:
        copy.start()
    blend_gate = jax.nn.sigmoid(
        jnp.sum(h_two.astype(F32) * mix_gate[...].astype(F32), axis=1, keepdims=True)
    )

    def dispatched(step, carry):
        ep_copy(
            0, step, disp_out.at[lax.rem(me_ep + step, n_ep)], disp_in.at[me_ep]
        ).wait()
        return carry

    for name in ("eg", "eu", "ed"):
        loads[name].wait()
    lax.fori_loop(1, n_ep, dispatched, 0)

    flat_rows = disp_in[...].astype(F32).reshape(rows, n_tp * width).astype(BF16)
    gate_pre = dot(flat_rows, eg[...])
    hidden = (gate_pre * jax.nn.sigmoid(gate_pre) * dot(flat_rows, eu[...])).astype(BF16)
    exp_copies = []
    for step in list(range(1, n_tp)) + [0]:
        target = lax.rem(me_tp + step, n_tp)
        columns = pl.ds(pl.multiple_of(target * width, width), width)
        exp_send[step] = dot(hidden, ed[:, columns]).astype(BF16)
        if step > 0:
            exp_copies.append(tp_copy(3, step, exp_send.at[step], exp_recv.at[step]))
            exp_copies[-1].start()
    dense_out = dense_send[me_tp].astype(F32)
    for step in range(1, n_tp):
        dense_copies[step - 1].wait()
        dense_out = dense_out + dense_recv[step].astype(F32)
    base = gathered[me_tp].astype(F32) + blend_gate * dense_out
    shares = exp_send[0].astype(F32)
    for step in range(1, n_tp):
        exp_copies[step - 1].wait()
        shares = shares + exp_recv[step].astype(F32)

    ret_out[...] = shares.reshape(n_ep, cap, width).astype(BF16)

    def give_back(step, carry):
        ep_copy(
            1, step, ret_out.at[lax.rem(me_ep + step, n_ep)], ret_in.at[me_ep]
        ).start()
        return carry

    lax.fori_loop(1, n_ep, give_back, 0)
    ret_in[me_ep] = ret_out[me_ep]

    def given_back(step, carry):
        ep_copy(
            1, step, ret_out.at[lax.rem(me_ep + step, n_ep)], ret_in.at[me_ep]
        ).wait()
        return carry

    lax.fori_loop(1, n_ep, given_back, 0)
    returned = ret_in[...].astype(F32).reshape(rows, width).astype(BF16)
    routed = dot(first, returned) * route_weight[:, 0:1]
    routed = routed + dot(second, returned) * route_weight[:, 1:2]
    out[...] = (base + routed).astype(BF16)


def local(
    n_ep,
    n_tp,
    tokens,
    kv_cache,
    cum_gate,
    lengths,
    w_query,
    w_key,
    w_value,
    w_forget,
    forget_bias,
    w_out,
    attn_gain,
    ffn_gain,
    mix_gate,
    expert_gate,
    expert_up,
    expert_down,
    chosen,
    route_weight,
    dense_gate,
    dense_up,
    dense_down,
):
    seqs, width = tokens.shape
    model = n_tp * width
    heads = w_query.shape[1] // HD
    assert w_key.shape[1] == HD
    cap = max(2, (4 * seqs + n_ep - 1) // n_ep)
    cap = (cap + 7) // 8 * 8
    rows = n_ep * cap
    vmem = pl.BlockSpec(memory_space=pltpu.VMEM)
    smem = pl.BlockSpec(memory_space=pltpu.SMEM)
    hbm = pl.BlockSpec(memory_space=pl.ANY)
    like = lambda a: pltpu.VMEM(a.shape, a.dtype)
    return pl.pallas_call(
        functools.partial(kernel, n_ep, n_tp, cap),
        out_shape=jax.ShapeDtypeStruct((seqs, width), BF16),
        in_specs=[vmem, smem] + [vmem] * 6 + [hbm] * 13,
        out_specs=vmem,
        scratch_shapes=[
            like(kv_cache),
            like(cum_gate),
            like(w_query),
            like(w_key),
            like(w_value),
            like(w_forget),
            like(w_out),
            like(expert_gate[0]),
            like(expert_up[0]),
            like(expert_down[0]),
            like(dense_gate),
            like(dense_up),
            like(dense_down),
            pltpu.SemaphoreType.DMA((12,)),
            pltpu.SemaphoreType.DMA((4,)),
            pltpu.VMEM((n_tp, seqs, width), BF16),
            pltpu.VMEM((seqs, heads, 2 * HD), F32),
            pltpu.VMEM((seqs, heads, 2 * HD), F32),
            pltpu.VMEM((seqs, 2 * HD), F32),
            pltpu.VMEM((seqs, heads, 2 * HD), F32),
            pltpu.VMEM((seqs, model), BF16),
            pltpu.VMEM((n_tp, seqs, model), BF16),
            pltpu.VMEM((n_ep, cap, model), BF16),
            pltpu.VMEM((n_ep, cap, model), BF16),
            pltpu.VMEM((n_tp, seqs, width), BF16),
            pltpu.VMEM((n_tp, seqs, width), BF16),
            pltpu.VMEM((n_tp, rows, width), BF16),
            pltpu.VMEM((n_tp, rows, width), BF16),
            pltpu.VMEM((n_ep, cap, width), BF16),
            pltpu.VMEM((n_ep, cap, width), BF16),
            pltpu.SemaphoreType.DMA((4, n_tp)),
            pltpu.SemaphoreType.DMA((4, n_tp)),
            pltpu.SemaphoreType.DMA((2, n_ep)),
            pltpu.SemaphoreType.DMA((2, n_ep)),
        ],
        compiler_params=pltpu.CompilerParams(
            collective_id=0,
            has_side_effects=True,
            vmem_limit_bytes=60 * 1024 * 1024,
        ),
    )(
        tokens,
        lengths,
        forget_bias.reshape(1, -1),
        attn_gain.reshape(1, -1),
        ffn_gain.reshape(1, -1),
        mix_gate.reshape(1, -1),
        chosen,
        route_weight,
        kv_cache,
        cum_gate,
        w_query,
        w_key,
        w_value,
        w_forget,
        w_out,
        expert_gate,
        expert_up,
        expert_down,
        dense_gate,
        dense_up,
        dense_down,
    )


def solution(mesh):
    in_specs = (
        P("ep", "tp"),
        P("ep", None, "tp"),
        P("ep", "tp", None),
        P("ep"),
        P(None, "tp"),
        P(None, "tp"),
        P(None, "tp"),
        P(None, "tp"),
        P("tp"),
        P("tp", None),
        P(),
        P(),
        P(),
        P("ep", None, "tp"),
        P("ep", None, "tp"),
        P("ep", "tp", None),
        P("ep", None),
        P("ep", None),
        P(None, "tp"),
        P(None, "tp"),
        P("tp", None),
    )
    out_specs = P("ep", "tp")
    return jax.shard_map(
        functools.partial(local, mesh.shape["ep"], mesh.shape["tp"]),
        mesh=mesh,
        in_specs=in_specs,
        out_specs=out_specs,
        check_vma=False,
    )
```

time: 131 us -> 54.9 us (0.42)
  waiting for transfers between devices: 69.4 us -> 0 us
  Pallas kernels: 0 us -> 40.7 us
  matrix products: 17.9 us -> 0 us
  between operations: 13.3 us -> 0.01 us
  starting transfers between devices: 11.1 us -> 0 us
  blocking collectives: 6.57 us -> 0 us
  local copies, waits for them, and re-layouts: 7.77 us -> 13.6 us
  other arithmetic: 4.38 us -> 0 us
    pallas_call x0 -> x1, Pallas kernels: none -> 40.7 us  [local(): pl.pallas_call(functools.partial(kernel, n_ep, n_tp, cap), out_shape=jax....]
    psum x1 -> x0, waiting for transfers between devices: 32.6 us -> none  [local(): lax.psum(partial_value.astype(jnp.bfloat16), 'tp').astype(jnp.float32)]
    reduce_scatter x2 -> x0, waiting for transfers between devices: 23.3 us -> none  [the longest x1 14.6 us: local(): lax.psum_scatter(part_out.astype(jnp.bfloat16), 'tp', scatter_dimension=1...]
    dot_general x15 -> x0, matrix products: 17.9 us -> none  [the longest x1 2.72 us: local(): jnp.dot(hidden, expert_down[0], preferred_element_type=jnp.float32)]
    all_to_all x2 -> x0, waiting for transfers between devices: 13.5 us -> none  [the longest x1 7.45 us: local(): lax.all_to_all(outgoing, 'ep', split_axis=0, concat_axis=0, tiled=True)]
    all_to_all x2 -> x0, starting transfers between devices: 11 us -> none  [the longest x1 5.52 us: local(): lax.all_to_all(outgoing, 'ep', split_axis=0, concat_axis=0, tiled=True)]
    all_gather x1 -> x0, blocking collectives: 6.57 us -> none  [local(): gathered = lax.all_gather(tokens, 'tp', axis=1, tiled=True)]
    reshape x2 -> x3, local copies, waits for them, and re-layouts: 0.18 us -> 3.86 us  [the longest x1 1.29 us: local(): attn_gain.reshape(1, -1)]
  transfers between devices with their start and end apart: 5 -> 0, of which waited for: 5 -> 0; matrix products, arithmetic and copies ran while one was open for 5% -> 0% of each run, Pallas kernels for 0% -> 0%
where the time goes in v1:
time: 54.9 us; the launch traced here: 54.4 us
  Pallas kernels  40.7 us (74%)
  local copies, waits for them, and re-layouts  13.6 us (25%)
    pallas_call x1, Pallas kernels, local(): pl.pallas_call(functools.partial(kernel, n_ep, n_tp, cap), out_shape=jax....  40.7 us
    unnamed x6, local copies, waits for them, and re-layouts  9.73 us
    reshape x1, local copies, waits for them, and re-layouts, local(): attn_gain.reshape(1, -1)  1.29 us
    reshape x1, local copies, waits for them, and re-layouts, local(): ffn_gain.reshape(1, -1)  1.29 us
    reshape x1, local copies, waits for them, and re-layouts, local(): mix_gate.reshape(1, -1)  1.29 us

profile of v1, /device:TPU:0, one launch (start us, length us, event | category | flops | bytes accessed | tf_op | source)
XLA Modules:
  0.0 54.4 jit_solution(2100181329439363202)
XLA Ops:
  0.0 1.3 %reshape.13.attn_gain = bf16[1,2048]{1,0:T(2,128)(2,1)} reshape(bf16[2048]{0:T(1024)(128)(2,1)} %param.31) | data formatting | bytes 8192 | tf_op jit(solution)/shard_map/reshape | solution.py:445
  1.3 1.3 %reshape.14.ffn_gain = bf16[1,2048]{1,0:T(2,128)(2,1)} reshape(bf16[2048]{0:T(1024)(128)(2,1)} %param.32) | data formatting | bytes 8192 | tf_op jit(solution)/shard_map/reshape | solution.py:446
  2.6 1.3 %reshape.15.mix_gate = bf16[1,2048]{1,0:T(2,128)(2,1)} reshape(bf16[2048]{0:T(1024)(128)(2,1)} %param.33) | data formatting | bytes 8192 | tf_op jit(solution)/shard_map/reshape | solution.py:447
  3.9 1.3 %copy.22.chosen = s32[16,2]{1,0:T(8,128)} copy(s32[16,2]{0,1:T(2,128)} %param.37) | data formatting | bytes 256 | tf_op args[16]
  5.2 1.3 %copy.23.route_weight = f32[16,2]{1,0:T(8,128)} copy(f32[16,2]{0,1:T(2,128)} %param.38) | data formatting | bytes 256 | tf_op args[17]
  6.6 1.9 %copy.24.wk_hbm = bf16[2048,64]{1,0:T(8,128)(2,1)} copy(bf16[2048,64]{0,1:T(8,128)(2,1)} %param.26) | data formatting | bytes 524288 | tf_op args[5]
  8.5 2.0 %copy.25.wv_hbm = bf16[2048,64]{1,0:T(8,128)(2,1)} copy(bf16[2048,64]{0,1:T(8,128)(2,1)} %param.27) | data formatting | bytes 524288 | tf_op args[6]
  10.5 1.8 %copy.26.wf_hbm = bf16[2048,4]{1,0:T(8,128)(2,1)} copy(bf16[2048,4]{0,1:T(4,128)(2,1)} %param.28) | data formatting | bytes 32768 | tf_op args[7]
  12.3 40.7 %shard_map.199 = bf16[16,512]{1,0:T(8,128)(2,1)} custom-call(bf16[16,512]{1,0:T(8,128)(2,1)} %tokens.1, s32[16]{0:T(128)} %lengths.1, f32[1,4]{1,0:T(1,128)} %bitcast.1, bf16[1,2048]{1,0:T(2,128)(2,1)} %reshape.13.attn_gain, bf16[1,2048]{1,0:T(2,128)(2,1)} %reshape.14.ffn_gain, bf16[1,2048]{1,0:T(2,128)(2,1)} %reshape.15.mix_gate, s32[16,2]{1,0:T(8,128)} %copy.22.chosen, ...), custom_call_target="tpu_custom_call" | custom-call | tf_op jit(solution)/shard_map/pallas_call | solution.py:395
  53.0 1.3 %copy.28 = bf16[16,512]{1,0:T(8,128)(2,1)} copy(bf16[16,512]{1,0:T(8,128)(2,1)} %shard_map.199) | data formatting | bytes 32768

commit v2 on v1

--- a/solution.py
+++ b/solution.py
@@ -17,6 +17,10 @@
 
 def dot(a, b):
     return jnp.dot(a, b, preferred_element_type=F32)
+
+
+def dot_t(a, b):
+    return lax.dot_general(a, b, (((1,), (1,)), ((), ())), preferred_element_type=F32)
 
 
 def norm_rows(widened, scales):
@@ -175,35 +179,39 @@
         copy.start()
     gathered[me_tp] = tokens[...]
 
-    slot = lax.broadcasted_iota(jnp.int32, (seqs, rows), 1)
+    slot = lax.broadcasted_iota(jnp.int32, (rows, seqs), 0)
     slot_expert = slot // cap
     slot_place = (slot % cap).astype(F32)
-    first = (chosen[:, 0:1] == slot_expert).astype(F32)
-    second = (chosen[:, 1:2] == slot_expert).astype(F32)
+    first = (chosen[0:1, :] == slot_expert).astype(F32)
+    second = (chosen[1:2, :] == slot_expert).astype(F32)
     either = first + second
     earlier = (
-        lax.broadcasted_iota(jnp.int32, (seqs, seqs), 1)
-        < lax.broadcasted_iota(jnp.int32, (seqs, seqs), 0)
+        lax.broadcasted_iota(jnp.int32, (seqs, seqs), 0)
+        < lax.broadcasted_iota(jnp.int32, (seqs, seqs), 1)
     ).astype(F32)
-    rank = dot(earlier.astype(BF16), either.astype(BF16))
+    rank = dot(either.astype(BF16), earlier.astype(BF16))
     in_place = (rank == slot_place).astype(F32)
-    first = (first * in_place).astype(BF16)
-    second = (second * in_place).astype(BF16)
-    either = either * in_place
+    either = (either * in_place).astype(BF16)
+    weighted = first * route_weight[0:1, :] + second * route_weight[1:2, :]
+    weighted = jnp.transpose(weighted * in_place)
+    high = weighted.astype(BF16).astype(F32)
+    middle = (weighted - high).astype(BF16).astype(F32)
+    low = weighted - high - middle
+    combine = jnp.concatenate([high, middle, low], axis=0).astype(BF16)
 
     for copy in token_copies:
         copy.wait()
     tokens_full = jnp.concatenate(
         [gathered[member].astype(F32) for member in range(n_tp)], axis=1
     )
-    h_one = norm_rows(tokens_full, attn_gain[...])
+    h_one = norm_rows(tokens_full, attn_gain[...].reshape(1, -1))
 
     for name in ("wq", "wk", "wv", "wf"):
         loads[name].wait()
     queries = dot(h_one, wq[...]).astype(BF16).astype(F32)
-    key_new = dot(h_one, wk[...]).astype(BF16).astype(F32)
-    value_new = dot(h_one, wv[...]).astype(BF16).astype(F32)
-    forget_pre = dot(h_one, wf[...]) + forget_bias[...]
+    key_new = dot_t(h_one, wk[...]).astype(BF16).astype(F32)
+    value_new = dot_t(h_one, wv[...]).astype(BF16).astype(F32)
+    forget_pre = dot_t(h_one, wf[...]) + forget_bias[...]
     forget_now = jnp.minimum(forget_pre, 0.0) - jnp.log1p(
         jnp.exp(-jnp.abs(forget_pre))
     )
@@ -266,11 +274,11 @@
         att_copies[step - 1].wait()
         attention = attention + att_in[step].astype(F32)
     residual_full = (tokens_full + attention).astype(BF16)
-    h_two = norm_rows(residual_full.astype(F32), ffn_gain[...])
+    h_two = norm_rows(residual_full.astype(F32), ffn_gain[...].reshape(1, -1))
     for member in range(n_tp):
         gathered[member] = residual_full[:, member * width : (member + 1) * width]
 
-    outgoing = dot(jnp.transpose(either).astype(BF16), h_two)
+    outgoing = dot(either, h_two)
     disp_out[...] = outgoing.reshape(n_ep, cap, n_tp * width).astype(BF16)
 
     def dispatch(step, carry):
@@ -298,7 +306,7 @@
     for copy in dense_copies:
         copy.start()
     blend_gate = jax.nn.sigmoid(
-        jnp.sum(h_two.astype(F32) * mix_gate[...].astype(F32), axis=1, keepdims=True)
+        jnp.sum(h_two.astype(F32) * mix_gate[...].reshape(1, -1).astype(F32), axis=1, keepdims=True)
     )
 
     def dispatched(step, carry):
@@ -351,8 +359,8 @@
 
     lax.fori_loop(1, n_ep, given_back, 0)
     returned = ret_in[...].astype(F32).reshape(rows, width).astype(BF16)
-    routed = dot(first, returned) * route_weight[:, 0:1]
-    routed = routed + dot(second, returned) * route_weight[:, 1:2]
+    routed = dot(combine, returned)
+    routed = routed[:seqs] + routed[seqs : 2 * seqs] + routed[2 * seqs :]
     out[...] = (base + routed).astype(BF16)
 
 
@@ -401,9 +409,9 @@
             like(kv_cache),
             like(cum_gate),
             like(w_query),
-            like(w_key),
-            like(w_value),
-            like(w_forget),
+            like(w_key.T),
+            like(w_value.T),
+            like(w_forget.T),
             like(w_out),
             like(expert_gate[0]),
             like(expert_up[0]),
@@ -442,17 +450,17 @@
         tokens,
         lengths,
         forget_bias.reshape(1, -1),
-        attn_gain.reshape(1, -1),
-        ffn_gain.reshape(1, -1),
-        mix_gate.reshape(1, -1),
-        chosen,
-        route_weight,
+        attn_gain,
+        ffn_gain,
+        mix_gate,
+        chosen.T,
+        route_weight.T,
         kv_cache,
         cum_gate,
         w_query,
-        w_key,
-        w_value,
-        w_forget,
+        w_key.T,
+        w_value.T,
+        w_forget.T,
         w_out,
         expert_gate,
         expert_up,

time: 54.9 us -> 42.4 us (0.77)
  local copies, waits for them, and re-layouts: 13.6 us -> 1.32 us
    unnamed x6 -> x1, local copies, waits for them, and re-layouts: 9.73 us -> 1.32 us
    reshape x3 -> x0, local copies, waits for them, and re-layouts: 3.86 us -> none  [the longest x1 1.29 us: local(): attn_gain.reshape(1, -1)]
where the time goes in v2:
time: 42.4 us; the launch traced here: 42.1 us
  Pallas kernels  40.7 us (96%)
  local copies, waits for them, and re-layouts  1.32 us (3%)
    pallas_call x1, Pallas kernels, local(): pl.pallas_call(functools.partial(kernel, n_ep, n_tp, cap), out_shape=jax....  40.7 us
    unnamed x1, local copies, waits for them, and re-layouts  1.32 us

profile of v2, /device:TPU:0, one launch (start us, length us, event | category | flops | bytes accessed | tf_op | source)
XLA Modules:
  0.0 42.1 jit_solution(6379637302347865950)
XLA Ops:
  0.0 40.7 %shard_map.199 = bf16[16,512]{1,0:T(8,128)(2,1)} custom-call(bf16[16,512]{1,0:T(8,128)(2,1)} %tokens.1, s32[16]{0:T(128)} %lengths.1, f32[1,4]{1,0:T(1,128)} %bitcast.11, bf16[2048]{0:T(1024)(128)(2,1)} %attn_gain.1, bf16[2048]{0:T(1024)(128)(2,1)} %ffn_gain.1, bf16[2048]{0:T(1024)(128)(2,1)} %mix_gate.1, s32[2,16]{1,0:T(2,128)} %bitcast.9, ...), custom_call_target="tpu_custom_call" | custom-call | tf_op jit(solution)/shard_map/pallas_call | solution.py:403
  40.8 1.3 %copy.23 = bf16[16,512]{1,0:T(8,128)(2,1)} copy(bf16[16,512]{1,0:T(8,128)(2,1)} %shard_map.199) | data formatting | bytes 32768

commit v3 on v2

--- a/solution.py
+++ b/solution.py
@@ -32,14 +32,14 @@
     n_ep,
     n_tp,
     cap,
-    tokens,
-    lengths,
-    forget_bias,
-    attn_gain,
-    ffn_gain,
-    mix_gate,
-    chosen,
-    route_weight,
+    tokens_hbm,
+    lengths_hbm,
+    forget_bias_hbm,
+    attn_gain_hbm,
+    ffn_gain_hbm,
+    mix_gate_hbm,
+    chosen_hbm,
+    route_weight_hbm,
     kv_hbm,
     cum_hbm,
     wq_hbm,
@@ -54,6 +54,15 @@
     du_hbm,
     dd_hbm,
     out,
+    tokens,
+    lengths,
+    forget_bias,
+    attn_gain,
+    ffn_gain,
+    mix_gate,
+    chosen,
+    route_weight,
+    small_sem,
     kv,
     cum,
     wq,
@@ -88,6 +97,8 @@
     tp_recv,
     ep_send,
     ep_recv,
+    relay_send,
+    relay_recv,
 ):
     me_tp = lax.axis_index("tp")
     me_ep = lax.axis_index("ep")
@@ -96,18 +107,45 @@
     cache_len = kv.shape[1]
     rows = n_ep * cap
 
+    barrier = pltpu.get_barrier_semaphore()
+    for step in range(1, n_tp):
+        pl.semaphore_signal(
+            barrier,
+            inc=1,
+            device_id={"tp": lax.rem(me_tp + step, n_tp)},
+            device_id_type=MESH,
+        )
+
+    def greet(step, carry):
+        pl.semaphore_signal(
+            barrier,
+            inc=1,
+            device_id={"ep": lax.rem(me_ep + step, n_ep)},
+            device_id_type=MESH,
+        )
+        return carry
+
+    lax.fori_loop(1, n_ep, greet, 0)
+
     loads = {}
-    for spot, (name, src, dst) in enumerate(
-        (
-            ("wq", wq_hbm, wq),
-            ("wk", wk_hbm, wk),
-            ("wv", wv_hbm, wv),
-            ("wf", wf_hbm, wf),
-            ("cum", cum_hbm, cum),
-        )
-    ):
-        loads[name] = pltpu.make_async_copy(src, dst, load_sem.at[spot])
+
+    def load(name, src, dst, sem):
+        loads[name] = pltpu.make_async_copy(src, dst, sem)
         loads[name].start()
+
+    load("tokens", tokens_hbm, tokens, small_sem.at[0])
+    load("attn_gain", attn_gain_hbm, attn_gain, small_sem.at[1])
+    load("chosen", chosen_hbm, chosen, small_sem.at[2])
+    load("route_weight", route_weight_hbm, route_weight, small_sem.at[3])
+    load("forget_bias", forget_bias_hbm, forget_bias, small_sem.at[4])
+    load("lengths", lengths_hbm, lengths, small_sem.at[5])
+    load("ffn_gain", ffn_gain_hbm, ffn_gain, small_sem.at[6])
+    load("mix_gate", mix_gate_hbm, mix_gate, small_sem.at[7])
+    load("wq", wq_hbm, wq, load_sem.at[0])
+    load("wk", wk_hbm, wk, load_sem.at[1])
+    load("wv", wv_hbm, wv, load_sem.at[2])
+    load("wf", wf_hbm, wf, load_sem.at[3])
+    load("cum", cum_hbm, cum, load_sem.at[4])
     kv_parts = kv_sem.shape[0]
     part = seqs // kv_parts
     kv_loads = []
@@ -117,39 +155,8 @@
             pltpu.make_async_copy(kv_hbm.at[span], kv.at[span], kv_sem.at[piece])
         )
         kv_loads[-1].start()
-    for spot, (name, src, dst) in enumerate(
-        (
-            ("wo", wo_hbm, wo),
-            ("dg", dg_hbm, dg),
-            ("du", du_hbm, du),
-            ("dd", dd_hbm, dd),
-            ("eg", eg_hbm.at[0], eg),
-            ("eu", eu_hbm.at[0], eu),
-            ("ed", ed_hbm.at[0], ed),
-        )
-    ):
-        loads[name] = pltpu.make_async_copy(src, dst, load_sem.at[5 + spot])
-        loads[name].start()
-
-    barrier = pltpu.get_barrier_semaphore()
-    for step in range(1, n_tp):
-        pl.semaphore_signal(
-            barrier,
-            inc=1,
-            device_id={"tp": lax.rem(me_tp + step, n_tp)},
-            device_id_type=MESH,
-        )
-
-    def greet(step, carry):
-        pl.semaphore_signal(
-            barrier,
-            inc=1,
-            device_id={"ep": lax.rem(me_ep + step, n_ep)},
-            device_id_type=MESH,
-        )
-        return carry
-
-    lax.fori_loop(1, n_ep, greet, 0)
+
+    loads["tokens"].wait()
     pl.semaphore_wait(barrier, n_tp - 1 + n_ep - 1)
 
     def tp_copy(phase, step, src, dst):
@@ -177,7 +184,18 @@
     ]
     for copy in token_copies:
         copy.start()
+    load("wo", wo_hbm, wo, load_sem.at[5])
+    load("dg", dg_hbm, dg, load_sem.at[6])
+    load("du", du_hbm, du, load_sem.at[7])
+    load("dd", dd_hbm, dd, load_sem.at[8])
+    load("eg", eg_hbm.at[0], eg, load_sem.at[9])
+    load("eu", eu_hbm.at[0], eu, load_sem.at[10])
+    load("ed", ed_hbm.at[0], ed, load_sem.at[11])
     gathered[me_tp] = tokens[...]
+    for name in ("attn_gain", "chosen", "route_weight", "forget_bias"):
+        loads[name].wait()
+    for name in ("lengths", "ffn_gain", "mix_gate"):
+        loads[name].wait()
 
     slot = lax.broadcasted_iota(jnp.int32, (rows, seqs), 0)
     slot_expert = slot // cap
@@ -279,16 +297,28 @@
         gathered[member] = residual_full[:, member * width : (member + 1) * width]
 
     outgoing = dot(either, h_two)
-    disp_out[...] = outgoing.reshape(n_ep, cap, n_tp * width).astype(BF16)
-
-    def dispatch(step, carry):
+    half = n_tp * width // 2
+    for side in range(2):
+        disp_out[side] = (
+            outgoing[:, side * half : (side + 1) * half]
+            .reshape(n_ep, cap, half)
+            .astype(BF16)
+        )
+    mine = lax.rem(me_tp, 2)
+    far_first = sorted(range(1, n_ep), key=lambda step: abs(step - n_ep // 2))
+    disp_copies = [
         ep_copy(
-            0, step, disp_out.at[lax.rem(me_ep + step, n_ep)], disp_in.at[me_ep]
-        ).start()
-        return carry
-
-    lax.fori_loop(1, n_ep, dispatch, 0)
-    disp_in[me_ep] = disp_out[me_ep]
+            0,
+            step,
+            disp_out.at[mine, lax.rem(me_ep + step, n_ep)],
+            disp_in.at[mine, me_ep],
+        )
+        for step in far_first
+    ]
+    for copy in disp_copies:
+        copy.start()
+    for side in range(2):
+        disp_in[side, me_ep] = disp_out[side, me_ep]
 
     for name in ("dg", "du", "dd"):
         loads[name].wait()
@@ -309,17 +339,31 @@
         jnp.sum(h_two.astype(F32) * mix_gate[...].reshape(1, -1).astype(F32), axis=1, keepdims=True)
     )
 
-    def dispatched(step, carry):
-        ep_copy(
-            0, step, disp_out.at[lax.rem(me_ep + step, n_ep)], disp_in.at[me_ep]
-        ).wait()
-        return carry
-
+    relays = []
+    for step, copy in reversed(list(zip(far_first, disp_copies))):
+        source = lax.rem(me_ep + n_ep - step, n_ep)
+        copy.wait_recv()
+        relays.append(
+            pltpu.make_async_remote_copy(
+                src_ref=disp_in.at[mine, source],
+                dst_ref=disp_in.at[mine, source],
+                send_sem=relay_send.at[step],
+                recv_sem=relay_recv.at[step],
+                device_id={"tp": me_tp + 1 - 2 * mine},
+                device_id_type=MESH,
+            )
+        )
+        relays[-1].start()
     for name in ("eg", "eu", "ed"):
         loads[name].wait()
-    lax.fori_loop(1, n_ep, dispatched, 0)
-
-    flat_rows = disp_in[...].astype(F32).reshape(rows, n_tp * width).astype(BF16)
+    for copy in disp_copies:
+        copy.wait_send()
+    for copy in relays:
+        copy.wait()
+
+    flat_rows = jnp.concatenate(
+        [disp_in[side].astype(F32).reshape(rows, half) for side in range(2)], axis=1
+    ).astype(BF16)
     gate_pre = dot(flat_rows, eg[...])
     hidden = (gate_pre * jax.nn.sigmoid(gate_pre) * dot(flat_rows, eu[...])).astype(BF16)
     exp_copies = []
@@ -342,22 +386,15 @@
 
     ret_out[...] = shares.reshape(n_ep, cap, width).astype(BF16)
 
-    def give_back(step, carry):
-        ep_copy(
-            1, step, ret_out.at[lax.rem(me_ep + step, n_ep)], ret_in.at[me_ep]
-        ).start()
-        return carry
-
-    lax.fori_loop(1, n_ep, give_back, 0)
+    ret_copies = [
+        ep_copy(1, step, ret_out.at[lax.rem(me_ep + step, n_ep)], ret_in.at[me_ep])
+        for step in far_first
+    ]
+    for copy in ret_copies:
+        copy.start()
     ret_in[me_ep] = ret_out[me_ep]
-
-    def given_back(step, carry):
-        ep_copy(
-            1, step, ret_out.at[lax.rem(me_ep + step, n_ep)], ret_in.at[me_ep]
-        ).wait()
-        return carry
-
-    lax.fori_loop(1, n_ep, given_back, 0)
+    for copy in ret_copies:
+        copy.wait()
     returned = ret_in[...].astype(F32).reshape(rows, width).astype(BF16)
     routed = dot(combine, returned)
     routed = routed[:seqs] + routed[seqs : 2 * seqs] + routed[2 * seqs :]
@@ -397,15 +434,23 @@
     cap = (cap + 7) // 8 * 8
     rows = n_ep * cap
     vmem = pl.BlockSpec(memory_space=pltpu.VMEM)
-    smem = pl.BlockSpec(memory_space=pltpu.SMEM)
     hbm = pl.BlockSpec(memory_space=pl.ANY)
     like = lambda a: pltpu.VMEM(a.shape, a.dtype)
     return pl.pallas_call(
         functools.partial(kernel, n_ep, n_tp, cap),
         out_shape=jax.ShapeDtypeStruct((seqs, width), BF16),
-        in_specs=[vmem, smem] + [vmem] * 6 + [hbm] * 13,
+        in_specs=[hbm] * 21,
         out_specs=vmem,
         scratch_shapes=[
+            like(tokens),
+            pltpu.SMEM(lengths.shape, lengths.dtype),
+            pltpu.VMEM((1, heads), F32),
+            like(attn_gain),
+            like(ffn_gain),
+            like(mix_gate),
+            like(chosen.T),
+            like(route_weight.T),
+            pltpu.SemaphoreType.DMA((8,)),
             like(kv_cache),
             like(cum_gate),
             like(w_query),
@@ -428,8 +473,8 @@
             pltpu.VMEM((seqs, heads, 2 * HD), F32),
             pltpu.VMEM((seqs, model), BF16),
             pltpu.VMEM((n_tp, seqs, model), BF16),
-            pltpu.VMEM((n_ep, cap, model), BF16),
-            pltpu.VMEM((n_ep, cap, model), BF16),
+            pltpu.VMEM((2, n_ep, cap, model // 2), BF16),
+            pltpu.VMEM((2, n_ep, cap, model // 2), BF16),
             pltpu.VMEM((n_tp, seqs, width), BF16),
             pltpu.VMEM((n_tp, seqs, width), BF16),
             pltpu.VMEM((n_tp, rows, width), BF16),
@@ -440,6 +485,8 @@
             pltpu.SemaphoreType.DMA((4, n_tp)),
             pltpu.SemaphoreType.DMA((2, n_ep)),
             pltpu.SemaphoreType.DMA((2, n_ep)),
+            pltpu.SemaphoreType.DMA((n_ep,)),
+            pltpu.SemaphoreType.DMA((n_ep,)),
         ],
         compiler_params=pltpu.CompilerParams(
             collective_id=0,

time: 42.4 us -> 41 us (0.967)
  Pallas kernels: 40.7 us -> 39.4 us
    pallas_call x1, Pallas kernels: 40.7 us -> 39.4 us  [local(): pl.pallas_call(functools.partial(kernel, n_ep, n_tp, cap), out_shape=jax....]
where the time goes in v3:
time: 41 us; the launch traced here: 40.8 us
  Pallas kernels  39.4 us (96%)
  local copies, waits for them, and re-layouts  1.32 us (3%)
    pallas_call x1, Pallas kernels, local(): pl.pallas_call(functools.partial(kernel, n_ep, n_tp, cap), out_shape=jax....  39.4 us
    unnamed x1, local copies, waits for them, and re-layouts  1.32 us

profile of v3, /device:TPU:0, one launch (start us, length us, event | category | flops | bytes accessed | tf_op | source)
XLA Modules:
  0.0 40.8 jit_solution(13005052866212943335)
XLA Ops:
  0.0 39.4 %shard_map.199 = bf16[16,512]{1,0:T(8,128)(2,1)} custom-call(bf16[16,512]{1,0:T(8,128)(2,1)} %tokens_hbm.1, s32[16]{0:T(128)} %lengths_hbm.1, f32[1,4]{1,0:T(1,128)} %bitcast.11, bf16[2048]{0:T(1024)(128)(2,1)} %attn_gain_hbm.1, bf16[2048]{0:T(1024)(128)(2,1)} %ffn_gain_hbm.1, bf16[2048]{0:T(1024)(128)(2,1)} %mix_gate_hbm.1, s32[2,16]{1,0:T(2,128)} %bitcast.9, ...), custom_call_target="tpu_custom_call" | custom-call | tf_op jit(solution)/shard_map/pallas_call | solution.py:439
  39.4 1.3 %copy.23 = bf16[16,512]{1,0:T(8,128)(2,1)} copy(bf16[16,512]{1,0:T(8,128)(2,1)} %shard_map.199) | data formatting | bytes 32768
